TPU v7x, 32 devices: a whole 2x2x4 slice. The times are simulated.
32 devices in a mesh: sp: 8 (over z, y), tp: 4 (over x, core).
Axes of the slice: x: 2, y: 2, z: 4, core: 2. Of those that a mesh axis runs over, the one named last changes fastest.
Arguments:
- inputs: bfloat16 [2, 1024, 2048], P(None, 'sp'), may hold values from -6 to 6
- norm_gain: float32 [2048], replicated, may hold values from 0.1 to 1.9
- query_weight: bfloat16 [2048, 1024], P('sp', 'tp'), may hold values from -0.125 to 0.125
- key_weight: bfloat16 [2048, 256], P('sp', 'tp'), may hold values from -0.125 to 0.125
- value_weight: bfloat16 [2048, 256], P('sp', 'tp'), may hold values from -0.125 to 0.125
- query_gain: float32 [64], replicated, may hold values from 0.1 to 24
- key_gain: float32 [64], replicated, may hold values from 0.1 to 1.9
- forget_cache: float32 [2, 16, 1024], P(None, 'tp'), may hold values from -104 to 0, as said below
- rec_in_weight: bfloat16 [2048, 1024], P('sp', 'tp'), may hold values from -0.125 to 0.125
- rec_gate_weight: bfloat16 [2048, 1024], P('sp', 'tp'), may hold values from -0.125 to 0.125
- conv_weight: bfloat16 [4, 1024], P(None, 'tp'), may hold values from -3 to 3
- decay_gate_weight: bfloat16 [16, 64, 64], P('tp'), may hold values from -0.75 to 0.75
- input_gate_weight: bfloat16 [16, 64, 64], P('tp'), may hold values from -0.75 to 0.75
- decay_param: float32 [1024], P('tp'), may hold values from 4 to 16
- decay_extra: float32 [2, 1024, 1024], P(None, 'sp', 'tp'), may hold values from -2 to 0
- attn_out_gain: float32 [1024], P('tp'), may hold values from 0.1 to 1.9
- rec_out_gain: float32 [1024], P('tp'), may hold values from 0.1 to 1.9
- out_att_weight: bfloat16 [1024, 2048], P('tp'), may hold values from -0.125 to 0.125
- out_rec_weight: bfloat16 [1024, 2048], P('tp'), may hold values from -0.125 to 0.125
Outputs:
- mixed: bfloat16 [2, 1024, 2048], P(None, 'sp', 'tp')
Inputs may be any that keep to these rules, and one draw needn't show every extreme that they name: `forget_cache`: Non-increasing along the positions of each sequence and head.
All inputs are finite; a program needn't handle non-finite values.
Results may differ from a plain program's by a relative error of at most 0.012.
The roundings to bfloat16 on the way count: a program that leaves them out, or rounds other values in their place, can miss the bound.
Values may be sent and summed in bfloat16 or wider, within the bound.
A program may use at most 128 MiB of HBM per device.

v0:
```python
import jax
import jax.numpy as jnp
from jax import lax
from jax.sharding import PartitionSpec as P

D = 2048
LRU_BLOCK = 64
CONV_TAPS = 4
lru_const = 8.0
norm_eps = 1e-06


def from_behind(value, axis, steps):
    count = lax.axis_size(axis)
    leading, last = (max(0, -steps), min(count, count - steps))
    return lax.ppermute(value, axis, [(source, source + steps) for source in range(leading, last)])


def rms_scale(values, gain):
    multiplier = lax.rsqrt(jnp.mean(values * values, axis=-1, keepdims=True) + norm_eps)
    return values * multiplier * gain


def merge_state(earlier, later):
    return (earlier[0] * later[0], later[0] * earlier[1] + later[1])


def block_length(length, span):
    shards = max(length // span, 1)
    group_size = 1
    for trial_size in range(1, shards + 1):
        if shards % trial_size == 0 and trial_size * span <= 1024:
            group_size = trial_size
    sub_size = group_size * span
    if length % sub_size:
        sub_size = length
    return sub_size


def body(
    inputs,
    norm_gain,
    query_weight,
    key_weight,
    value_weight,
    query_gain,
    key_gain,
    forget_cache,
    rec_in_weight,
    rec_gate_weight,
    conv_weight,
    decay_gate_weight,
    input_gate_weight,
    decay_param,
    decay_extra,
    attn_out_gain,
    rec_out_gain,
    out_att_weight,
    out_rec_weight,
):
    seq_count, seq_span, model_width = inputs.shape
    row_count = seq_count * seq_span
    head_dim = query_gain.shape[0]
    att_local = query_weight.shape[1] // head_dim
    kv_local = key_weight.shape[1] // head_dim
    head_group = att_local // kv_local
    channels = rec_in_weight.shape[1]
    normed = rms_scale(
        inputs.reshape(row_count, model_width).astype(jnp.float32), norm_gain
    ).astype(jnp.bfloat16)
    normed_cols = normed.T
    row_contract = (((0,), (0,)), ((), ()))
    kv_cols = key_weight.shape[1]
    pieces = (
        lax.all_gather(query_weight, "sp", axis=0, tiled=True),
        lax.all_gather(key_weight, "sp", axis=0, tiled=True),
        lax.all_gather(value_weight, "sp", axis=0, tiled=True),
        lax.all_gather(rec_in_weight, "sp", axis=0, tiled=True),
        lax.all_gather(rec_gate_weight, "sp", axis=0, tiled=True),
    )
    query_proj, key_proj, value_sum, rec_in_sum, gate_proj = tuple(
        (
            lax.dot_general(
                normed_cols, weight_part, row_contract, preferred_element_type=jnp.float32
            )
            for weight_part in pieces
        )
    )
    queries = rms_scale(query_proj.reshape(row_count, att_local, head_dim), query_gain).astype(
        jnp.bfloat16
    )
    queries = queries.reshape(seq_count, seq_span, kv_local, head_group, head_dim).transpose(
        0, 2, 3, 1, 4
    )
    queries = queries.reshape(seq_count, kv_local, head_group * seq_span, head_dim)
    key_heads = rms_scale(key_proj.reshape(row_count, kv_local, head_dim), key_gain).astype(
        jnp.bfloat16
    )
    key_heads = key_heads.reshape(seq_count, seq_span, kv_cols)
    value_heads = value_sum.astype(jnp.bfloat16).reshape(seq_count, seq_span, kv_cols)
    key_value = jnp.concatenate([key_heads, value_heads], axis=2)
    my_first = lax.axis_index("sp") * seq_span
    own_gates = lax.dynamic_slice_in_dim(forget_cache, my_first, seq_span, 2)
    own_gates = own_gates.reshape(seq_count, kv_local, head_group, seq_span, 1)
    query_pos = my_first + jnp.tile(jnp.arange(seq_span, dtype=jnp.int32), head_group)
    scaling = head_dim ** (-0.5)
    start_state = (
        jnp.full((seq_count, kv_local, head_group * seq_span), -jnp.inf, jnp.float32),
        jnp.zeros((seq_count, kv_local, head_group * seq_span), jnp.float32),
        jnp.zeros((seq_count, kv_local, head_group * seq_span, head_dim), jnp.float32),
    )
    shard_part = lax.all_gather(key_value, "sp", axis=1, tiled=True)
    offset = jnp.int32(0)
    length = shard_part.shape[1]
    sub_size = block_length(length, seq_span)

    def one_step(block_index, carried_state):
        key_first = offset + block_index * sub_size

        def work(carried):
            top_score, totals, accum = carried
            block_rows = lax.dynamic_slice_in_dim(shard_part, block_index * sub_size, sub_size, 1)
            key_block = block_rows[:, :, :kv_cols].reshape(seq_count, sub_size, kv_local, head_dim)
            value_block = block_rows[:, :, kv_cols:].reshape(
                seq_count, sub_size, kv_local, head_dim
            )
            key_gates = lax.dynamic_slice_in_dim(forget_cache, key_first, sub_size, 2)
            key_gates = key_gates.reshape(seq_count, kv_local, head_group, 1, sub_size)
            scores = (
                jnp.einsum(
                    "bhqd,bkhd->bhqk", queries, key_block, preferred_element_type=jnp.float32
                )
                * scaling
            )
            scores = (
                scores.reshape(seq_count, kv_local, head_group, seq_span, sub_size)
                + own_gates
                - key_gates
            )
            scores = scores.reshape(seq_count, kv_local, head_group * seq_span, sub_size)
            visible = (
                query_pos[:, None] >= (key_first + jnp.arange(sub_size, dtype=jnp.int32))[None, :]
            )
            scores = jnp.where(visible, scores, -jnp.inf)
            new_top = jnp.maximum(top_score, jnp.max(scores, axis=-1))
            safe_top = jnp.where(jnp.isfinite(new_top), new_top, 0.0)
            weights = jnp.exp(scores - safe_top[..., None])
            fading = jnp.exp(top_score - safe_top)
            totals = totals * fading + jnp.sum(weights, axis=-1)
            accum = accum * fading[..., None] + jnp.einsum(
                "bhqk,bkhd->bhqd",
                weights.astype(jnp.bfloat16),
                value_block,
                preferred_element_type=jnp.float32,
            )
            return (new_top, totals, accum)

        return lax.cond(
            key_first < my_first + seq_span, work, lambda carried: carried, carried_state
        )

    top_score, totals, accum = lax.fori_loop(0, length // sub_size, one_step, start_state)
    attended = (accum / totals[..., None]).reshape(
        seq_count, kv_local, head_group, seq_span, head_dim
    )
    attended = attended.transpose(0, 3, 1, 2, 4).reshape(row_count, att_local, head_dim)
    att_normed = rms_scale(attended, attn_out_gain.reshape(att_local, head_dim)).astype(
        jnp.bfloat16
    )
    att_normed = att_normed.reshape(row_count, att_local * head_dim)
    rec_in = rec_in_sum.astype(jnp.bfloat16).reshape(seq_count, seq_span, channels)
    before = from_behind(rec_in[:, seq_span - (CONV_TAPS - 1) :, :], "sp", 1)
    extended = jnp.concatenate([before, rec_in], axis=1)
    conv = jnp.zeros((seq_count, seq_span, channels), jnp.float32)
    for tap in range(CONV_TAPS):
        conv = conv + extended[:, tap : tap + seq_span].astype(jnp.float32) * conv_weight[
            tap
        ].astype(jnp.float32)
    conv = conv.astype(jnp.bfloat16)
    blocks_local = decay_gate_weight.shape[0]
    grouped = conv.reshape(seq_count, seq_span, blocks_local, LRU_BLOCK)
    gate_decay = jnp.einsum(
        "bsnd,nde->bsne", grouped, decay_gate_weight, preferred_element_type=jnp.float32
    ).reshape(seq_count, seq_span, channels)
    gate_input = jnp.einsum(
        "bsnd,nde->bsne", grouped, input_gate_weight, preferred_element_type=jnp.float32
    ).reshape(seq_count, seq_span, channels)
    log_decay = (
        -lru_const * jax.nn.sigmoid(gate_decay) * jax.nn.softplus(-decay_param) + decay_extra
    )
    drive = (
        jnp.sqrt(-jnp.expm1(2.0 * log_decay))
        * jax.nn.sigmoid(gate_input)
        * conv.astype(jnp.float32)
    )
    cum_decay, local_state = lax.associative_scan(merge_state, (jnp.exp(log_decay), drive), axis=1)
    every_decay, every_state = (
        lax.all_gather(cum_decay[:, seq_span - 1][None], "sp", axis=0, tiled=True),
        lax.all_gather(local_state[:, seq_span - 1][None], "sp", axis=0, tiled=True),
    )
    prefix_decay, prefix_state = lax.associative_scan(
        merge_state, (every_decay, every_state), axis=0
    )
    position = lax.axis_index("sp")
    earlier_state = lax.dynamic_index_in_dim(
        prefix_state, jnp.maximum(position - 1, 0), 0, keepdims=False
    )
    entering = jnp.where(position > 0, earlier_state, 0.0)
    state = local_state + cum_decay * entering[:, None, :]
    gated = state * jax.nn.gelu(gate_proj.reshape(seq_count, seq_span, channels))
    rec_normed = rms_scale(
        gated.reshape(row_count, blocks_local, LRU_BLOCK),
        rec_out_gain.reshape(blocks_local, LRU_BLOCK),
    ).astype(jnp.bfloat16)
    rec_normed = rec_normed.reshape(row_count, channels)
    out_cols = D // lax.axis_size("tp")
    pieces = row_count * lax.axis_size("tp") // row_count
    terms = jnp.dot(att_normed, out_att_weight, preferred_element_type=jnp.float32) + jnp.dot(
        rec_normed, out_rec_weight, preferred_element_type=jnp.float32
    )
    mixed_cols = lax.psum_scatter(
        terms.reshape(row_count, pieces, out_cols)
        .transpose(1, 0, 2)
        .reshape(pieces * row_count, out_cols)
        .astype(jnp.bfloat16),
        "tp",
        scatter_dimension=0,
        tiled=True,
    )
    return mixed_cols.reshape(seq_count, seq_span, out_cols)


def solution(mesh):
    return jax.shard_map(
        body,
        mesh=mesh,
        in_specs=(
            P(None, "sp", None),
            P(),
            P("sp", "tp"),
            P("sp", "tp"),
            P("sp", "tp"),
            P(),
            P(),
            P(None, "tp", None),
            P("sp", "tp"),
            P("sp", "tp"),
            P(None, "tp"),
            P("tp", None, None),
            P("tp", None, None),
            P("tp"),
            P(None, "sp", "tp"),
            P("tp"),
            P("tp"),
            P("tp", None),
            P("tp", None),
        ),
        out_specs=P(None, "sp", "tp"),
        check_vma=False,
    )
```

profile of v0, /device:TPU:0, one launch (start us, length us, event | category | flops | bytes accessed | tf_op | source)
XLA Modules:
  0.0 263.9 jit_solution(10849590766930557368)
XLA Ops:
  9.5 1.5 multiply_reduce_fusion
  11.0 1.4 slice_convert_fusion.3
  12.4 33.4 %all_gather.25 = bf16[2048,64]{0,1:T(8,128)(2,1)S(1)} all-gather(bf16[256,64]{0,1:T(8,128)(2,1)} %param.24), channel_id=1, replica_groups=mesh['sp'=8,'tp'=4] {'sp'}, dimensions={0}, use_global_device_ids=true | all-gather | bytes 294912 | tf_op jit(solution)/shard_map/all_gather | solution.py:76
  45.8 31.4 %all_gather.26 = bf16[2048,64]{0,1:T(8,128)(2,1)S(1)} all-gather(bf16[256,64]{0,1:T(8,128)(2,1)} %param.25), channel_id=1, replica_groups=mesh['sp'=8,'tp'=4] {'sp'}, dimensions={0}, use_global_device_ids=true | all-gather | bytes 294912 | tf_op jit(solution)/shard_map/all_gather | solution.py:77
  77.2 1.0 fusion.14
  79.3 29.7 %all_gather.27 = bf16[2,1024,128]{1,2,0:T(8,128)(2,1)} all-gather(bf16[2,128,128]{1,2,0:T(8,128)(2,1)S(1)} %pad_maximum_fusion.3), channel_id=1, replica_groups=mesh['sp'=8,'tp'=4] {'sp'}, dimensions={1}, use_global_device_ids=true | all-gather | bytes 589824 | tf_op jit(solution)/shard_map/all_gather | solution.py:112
  108.9 1.3 multiply_convert_fusion
  110.3 2.4 copy.49
  112.6 1.7 multiply_reduce_fusion.1
  114.6 6.3 %conditional.1 = ((f32[2,1,512]{2,0,1:T(2,128)S(1)}, f32[2,1,512,64]{2,3,0,1:T(8,128)S(1)})) conditional(s32[]{:T(128)} %convert_element_type.124, (f32[2,1,512]{2,0,1:T(2,128)S(1)}, f32[2,1,512,64]{2,3,0,1:T(8,128)S(1)}) %tuple.30, (s32[]{:T(128)}, s32[4,128]{1,0:T(4,128)S(1)}, bf16[2,1,4,128,64]{3,2,4,0,1:T(4,128)(2,1)S(1)}, ...), branch_computations={%region_3.4_spmd, %region_4.7_spmd} | conditional | flops 281680384 | bytes 17967226 | solution.py:158
  114.7 0.8 dynamic-slice_bitcast_fusion
  115.9 2.4 fusion.3
  118.4 1.8 fusion.1
  120.2 0.8 fusion.4
  121.5 1.7 convolution_convert_fusion
  123.3 3.3 %collective-permute-start = (bf16[2,3,256]{2,1,0:T(4,128)(2,1)S(1)}, bf16[2,3,256]{2,1,0:T(4,128)(2,1)S(1)}, u32[]{:S(2)}, u32[]{:S(2)}) collective-permute-start(bf16[2,3,256]{2,1,0:T(4,128)(2,1)S(1)} %slice.399), channel_id=1, source_target_pairs={{0,4},{4,8},{8,12},{12,16},{16,20},{20,24},{24,28},{1,5},{5,9},{9,... | collective-permute-start | bytes 9224 | tf_op jit(solution)/shard_map/ppermute | solution.py:16
  129.1 0.8 copy.62
  129.9 1.2 fusion.22
  131.1 0.8 copy.58
  132.0 2.0 convert_multiply_fusion
  134.7 1.6 slice.363
  136.4 1.0 slice.317
  137.3 1.6 slice.316
  141.6 1.1 multiply_add_fusion.1
  147.7 0.8 fusion.53
  149.2 0.8 pad.128
  151.9 0.9 pad_maximum_fusion.4
  152.8 2.1 pad.116
  154.9 0.8 pad.130
  155.7 1.6 add.383
  157.3 1.7 fusion.45
  159.0 1.5 pad.117
  160.5 2.3 pad.118
  162.8 0.7 slice_add_fusion.4
  163.6 26.3 %all-gather = f32[16,1,256]{2,1,0:T(1,128)S(1)} all-gather(f32[2,1,256]{2,1,0:T(1,128)S(1)} %slice_add_fusion.4), channel_id=2, replica_groups=mesh['sp'=8,'tp'=4] {'sp'}, dimensions={0}, use_global_device_ids=true | all-gather | bytes 18432 | tf_op jit(solution)/shard_map/all_gather | solution.py:199
  190.4 1.6 pad_maximum_fusion.2
  192.0 0.9 pad.131
  193.6 0.7 reshape.378
  194.3 1.2 copy.63
  195.6 1.4 pad.132
  197.7 26.1 %all-gather.1 = f32[16,1,256]{2,1,0:T(1,128)S(1)} all-gather(f32[2,1,256]{2,1,0:T(1,128)S(1)} %slice_add_fusion.3), channel_id=3, replica_groups=mesh['sp'=8,'tp'=4] {'sp'}, dimensions={0}, use_global_device_ids=true | all-gather | bytes 18432 | tf_op jit(solution)/shard_map/all_gather | solution.py:198
  224.9 3.0 %fusion.73 = (f32[2,128,256]{2,1,0:T(8,128)}, f32[2,128,256]{2,1,0:T(8,128)}) fusion(bf16[2,128,2048]{2,1,0:T(8,128)(2,1)} %multiply_convert_fusion, bf16[2048,256]{1,0:T(8,128)(2,1)} %all-gather.10.cloned.1.call-done, f32[2,256]{1,0:T(2,128)S(1)} %fusion.65, f32[2,128,256]{2,1,0:T(8,128)S(1)} %pad.131, f32[2,128,256]{2,1,0:T(8,128)} %pad.132, ...), kind=kOutput, calls=%fused_computation.170 | convolution fusion | flops 269352960 | bytes 3672064 | tf_op jit(solution)/shard_map/dot_general | solution.py:83
  227.9 1.8 copy.64
  229.7 1.2 mul.431
  230.9 1.1 copy.65
  232.1 1.7 fusion.12
  233.8 1.1 copy.94
  234.9 22.5 %reduce-scatter.2.cloned.1.call-done = bf16[256,512]{1,0:T(8,128)(2,1)} async-done(((bf16[1024,512]{1,0:T(8,128)(2,1)}), bf16[256,512]{1,0:T(8,128)(2,1)}) %reduce-scatter.2.cloned.1.call-update) | async-done | bytes 262160 | tf_op jit(solution)/shard_map/reduce_scatter | solution.py:221
  (192 shorter events, 21.6 us)
Async XLA Ops:
  6.5 120.2 %copy-start = (bf16[256,2048]{1,0:T(8,128)(2,1)S(1)}, bf16[256,2048]{1,0:T(8,128)(2,1)}, u32[]{:S(2)}) copy-start(bf16[256,2048]{1,0:T(8,128)(2,1)} %param.38) | copy-start | bytes 3145732
  6.5 70.7 %copy-start.1 = (bf16[2,128,2048]{2,1,0:T(8,128)(2,1)S(1)}, bf16[2,128,2048]{2,1,0:T(8,128)(2,1)}, u32[]{:S(2)}) copy-start(bf16[2,128,2048]{2,1,0:T(8,128)(2,1)} %param.21) | copy-start | bytes 3145732
  6.5 103.7 %all-gather.6.cloned.1.call-start = ((), (), s32[]{:S(2)}) async-start(), calls=%async_computation.1 | async-start | bytes 1179648 | tf_op jit(solution)/shard_map/all_gather | solution.py:75
  7.3 114.3 %all-gather.8.cloned.1.call-start = ((), (), s32[]{:S(2)}) async-start(), calls=%async_computation.2 | async-start | bytes 1179648 | tf_op jit(solution)/shard_map/all_gather | solution.py:78
  8.0 216.8 %all-gather.10.cloned.1.call-start = ((), (), s32[]{:S(2)}) async-start(), calls=%async_computation.3 | async-start | bytes 1179648 | tf_op jit(solution)/shard_map/all_gather | solution.py:79
  8.7 248.6 %reduce-scatter.2.cloned.1.call-start = ((), (), s32[]{:S(2)}) async-start(), calls=%async_computation.4 | async-start | bytes 1310720 | tf_op jit(solution)/shard_map/reduce_scatter | solution.py:221
  77.2 2.0 copy-start.15
  78.2 30.7 %copy-start.8 = (f32[2048]{0:T(1024)S(1)}, f32[2048]{0:T(1024)}, u32[]{:S(2)}) copy-start(f32[2048]{0:T(1024)} %param.22) | copy-start | bytes 24580
  110.2 2.4 copy-start.2
  112.6 1.7 copy-start.16
  115.9 2.5 copy-start.6
  118.3 1.8 copy-start.3
  121.0 5.6 %copy-start.13 = (f32[256]{0:T(256)S(1)}, f32[256]{0:T(256)}, u32[]{:S(2)}) copy-start(f32[256]{0:T(256)} %param.36) | copy-start | bytes 3076
  123.2 4.6 %copy-start.9 = (f32[1,256]{1,0:T(1,128)S(1)}, f32[1,256]{1,0:T(1,128)}, u32[]{:S(2)}) copy-start(f32[1,256]{1,0:T(1,128)} %get-tuple-element.199) | copy-start | bytes 3076
  123.2 4.6 %copy-start.10 = (f32[1,256]{1,0:T(1,128)S(1)}, f32[1,256]{1,0:T(1,128)}, u32[]{:S(2)}) copy-start(f32[1,256]{1,0:T(1,128)} %get-tuple-element.200) | copy-start | bytes 3076
  123.2 4.6 %copy-start.11 = (f32[1,256]{1,0:T(1,128)S(1)}, f32[1,256]{1,0:T(1,128)}, u32[]{:S(2)}) copy-start(f32[1,256]{1,0:T(1,128)} %get-tuple-element.201) | copy-start | bytes 3076
  123.2 4.6 %copy-start.12 = (f32[1,256]{1,0:T(1,128)S(1)}, f32[1,256]{1,0:T(1,128)}, u32[]{:S(2)}) copy-start(f32[1,256]{1,0:T(1,128)} %get-tuple-element.202) | copy-start | bytes 3076
  123.3 4.6 %collective-permute-start = (bf16[2,3,256]{2,1,0:T(4,128)(2,1)S(1)}, bf16[2,3,256]{2,1,0:T(4,128)(2,1)S(1)}, u32[]{:S(2)}, u32[]{:S(2)}) collective-permute-start(bf16[2,3,256]{2,1,0:T(4,128)(2,1)S(1)} %slice.399), channel_id=1, source_target_pairs={{0,4},{4,8},{8,12},{12,16},{16,20},{20,24},{24,28},{1,5},{5,9},{9,... | collective-permute-start | bytes 9224 | tf_op jit(solution)/shard_map/ppermute | solution.py:16
  126.6 2.2 copy-start.17
  128.1 0.7 copy-start.7
  144.1 7.1 %copy-start.4 = (f32[2,31,256]{2,1,0:T(8,128)S(1)}, f32[2,31,256]{2,1,0:T(8,128)}, u32[]{:S(2)}) copy-start(f32[2,31,256]{2,1,0:T(8,128)} %slice.361) | copy-start | bytes 190468
  144.2 7.1 %copy-start.5 = (f32[2,31,256]{2,1,0:T(8,128)S(1)}, f32[2,31,256]{2,1,0:T(8,128)}, u32[]{:S(2)}) copy-start(f32[2,31,256]{2,1,0:T(8,128)} %slice.320) | copy-start | bytes 190468
  224.8 7.1 %copy-start.14 = (f32[256]{0:T(256)S(1)}, f32[256]{0:T(256)}, u32[]{:S(2)}) copy-start(f32[256]{0:T(256)} %param.37) | copy-start | bytes 3076
Sparse Core Ops, SparseCore 0:
  9.5 44.2 all-gather.5
  55.9 41.5 all-gather.7
  99.6 38.9 all-gather.9
  235.0 22.3 reduce-scatter.1
where the time goes:
time: 265 us; the launch traced here: 264 us
  blocking collectives  147 us (55%)
  local copies, waits for them, and re-layouts  35.4 us (13%)
  waiting for transfers between devices  25.4 us (10%)
  other arithmetic  24.8 us (9%)
  matrix products  14.1 us (5%)
  between operations  13.9 us (5%)
  starting transfers between devices  3.38 us (1%)
    all_gather x1, blocking collectives, body(): lax.all_gather(key_weight, 'sp', axis=0, tiled=True)  33.4 us
    all_gather x1, blocking collectives, body(): lax.all_gather(value_weight, 'sp', axis=0, tiled=True)  31.4 us
    all_gather x1, blocking collectives, body(): shard_part = lax.all_gather(key_value, 'sp', axis=1, tiled=True)  29.7 us
    all_gather x1, blocking collectives, body(): lax.all_gather(local_state[:, seq_span - 1][None], 'sp', axis=0, tiled=True)  26.3 us
    all_gather x1, blocking collectives, body(): lax.all_gather(cum_decay[:, seq_span - 1][None], 'sp', axis=0, tiled=True)  26.1 us
    reduce_scatter x1, waiting for transfers between devices, body(): lax.psum_scatter(terms.reshape(row_count, pieces, out_cols).transpose(1,...  22.5 us
    slice x44, local copies, waits for them, and re-layouts, body(): lax.associative_scan(merge_state, (jnp.exp(log_decay), drive), axis=1)  11.2 us
    pad x24, local copies, waits for them, and re-layouts, body(): lax.associative_scan(merge_state, (jnp.exp(log_decay), drive), axis=1)  10.2 us
  transfers between devices with their start and end apart: 5, of which 2 were waited for; matrix products, arithmetic and copies ran while one was open for 24% of the time, Pallas kernels for 0%

commit v1 on v0

--- a/solution.py
+++ b/solution.py
@@ -8,6 +8,28 @@
 CONV_TAPS = 4
 lru_const = 8.0
 norm_eps = 1e-06
+
+
+def laid_out(parts, dim):
+    parts = jnp.moveaxis(parts, 0, dim)
+    lengths = parts.shape
+    return parts.reshape(*lengths[:dim], lengths[dim] * lengths[dim + 1], *lengths[dim + 2 :])
+
+
+def collected_by_bits(x, axis):
+    size = lax.axis_size(axis)
+    blocks = x[None]
+    for level in range(size.bit_length() - 1):
+        apart = 1 << level
+        theirs = lax.ppermute(blocks, axis, [(i, i ^ apart) for i in range(size)])
+        both = jnp.stack([blocks, theirs])
+        upper = lax.axis_index(axis) >> level & 1
+        blocks = jnp.where(upper == 0, both, both[::-1]).reshape(-1, *x.shape)
+    return blocks
+
+
+def doubled_up(shard, axis, dim):
+    return laid_out(collected_by_bits(shard, axis), dim)
 
 
 def from_behind(value, axis, steps):
@@ -74,7 +96,7 @@
     pieces = (
         lax.all_gather(query_weight, "sp", axis=0, tiled=True),
         lax.all_gather(key_weight, "sp", axis=0, tiled=True),
-        lax.all_gather(value_weight, "sp", axis=0, tiled=True),
+        doubled_up(value_weight, "sp", 0),
         lax.all_gather(rec_in_weight, "sp", axis=0, tiled=True),
         lax.all_gather(rec_gate_weight, "sp", axis=0, tiled=True),
     )

time: 265 us -> 210 us (0.79)
  blocking collectives: 147 us -> 115 us
  local copies, waits for them, and re-layouts: 35.4 us -> 15.5 us
  other arithmetic: 24.8 us -> 10.8 us
  waiting for transfers between devices: 25.4 us -> 35.2 us
    all_gather x1 -> x0, blocking collectives: 31.4 us -> none  [body(): lax.all_gather(value_weight, 'sp', axis=0, tiled=True)]
    ppermute x0 -> x3, waiting for transfers between devices: none -> 11.2 us  [collected_by_bits(): theirs = lax.ppermute(blocks, axis, [(i, i ^ apart) for i in range(size)])]
    slice x44, local copies, waits for them, and re-layouts: 11.2 us -> 0.95 us  [body(): lax.associative_scan(merge_state, (jnp.exp(log_decay), drive), axis=1)]
    pad x24, local copies, waits for them, and re-layouts: 10.2 us -> 0.78 us  [body(): lax.associative_scan(merge_state, (jnp.exp(log_decay), drive), axis=1)]
    add x13, other arithmetic: 4.97 us -> 0.13 us  [body(): lax.associative_scan(merge_state, (jnp.exp(log_decay), drive), axis=1)]
    add x13, other arithmetic: 4.34 us -> 0.24 us  [merge_state(): return (earlier[0] * later[0], later[0] * earlier[1] + later[1])]
    ppermute x0 -> x3, starting transfers between devices: none -> 3.2 us  [collected_by_bits(): theirs = lax.ppermute(blocks, axis, [(i, i ^ apart) for i in range(size)])]
    concatenate x11, other arithmetic: 3.16 us -> 0.12 us  [body(): lax.associative_scan(merge_state, (jnp.exp(log_decay), drive), axis=1)]
  transfers between devices with their start and end apart: 5 -> 8, of which waited for: 2 -> 3; matrix products, arithmetic and copies ran while one was open for 24% -> 13% of each run, Pallas kernels for 0% -> 0%
where the time goes in v1:
time: 210 us; the launch traced here: 209 us
  blocking collectives  115 us (55%)
  waiting for transfers between devices  35.2 us (17%)
  local copies, waits for them, and re-layouts  15.5 us (7%)
  between operations  14.3 us (7%)
  matrix products  12.8 us (6%)
  other arithmetic  10.8 us (5%)
  starting transfers between devices  5.71 us (3%)
    all_gather x1, blocking collectives, body(): lax.all_gather(key_weight, 'sp', axis=0, tiled=True)  32 us
    all_gather x1, blocking collectives, body(): shard_part = lax.all_gather(key_value, 'sp', axis=1, tiled=True)  30.3 us
    all_gather x1, blocking collectives, body(): lax.all_gather(local_state[:, seq_span - 1][None], 'sp', axis=0, tiled=True)  26.2 us
    all_gather x1, blocking collectives, body(): lax.all_gather(cum_decay[:, seq_span - 1][None], 'sp', axis=0, tiled=True)  26.1 us
    reduce_scatter x1, waiting for transfers between devices, body(): lax.psum_scatter(terms.reshape(row_count, pieces, out_cols).transpose(1,...  22.5 us
    ppermute x3, waiting for transfers between devices, collected_by_bits(): theirs = lax.ppermute(blocks, axis, [(i, i ^ apart) for i in range(size)])  11.2 us
    dot_general x5, matrix products, body(): lax.dot_general(normed_cols, weight_part, row_contract, preferred_element...  5.54 us
  transfers between devices with their start and end apart: 8, of which 3 were waited for; matrix products, arithmetic and copies ran while one was open for 13% of the time, Pallas kernels for 0%

profile of v1, /device:TPU:0, one launch (start us, length us, event | category | flops | bytes accessed | tf_op | source)
XLA Modules:
  0.0 209.0 jit_solution(6152858000602536622)
XLA Ops:
  6.5 0.7 all-gather.6.cloned.1.call-update
  7.3 0.7 all-gather.8.cloned.1.call-update
  8.1 3.1 %collective-permute-start = (bf16[1,256,64]{1,2,0:T(8,128)(2,1)}, bf16[1,256,64]{1,2,0:T(8,128)(2,1)S(1)}, u32[]{:S(2)}, u32[]{:S(2)}) collective-permute-start(bf16[1,256,64]{1,2,0:T(8,128)(2,1)} %bitcast.200), channel_id=1, source_target_pairs={{0,4},{4,0},{8,12},{12,8},{16,20},{20,16},{24,28},{28,24},{1,5},{5... | collective-permute-start | bytes 98312 | tf_op jit(solution)/shard_map/ppermute | solution.py:24
  11.2 1.5 multiply_reduce_fusion
  12.7 32.0 %all_gather.22 = bf16[2048,64]{0,1:T(8,128)(2,1)S(1)} all-gather(bf16[256,64]{0,1:T(8,128)(2,1)} %param.24), channel_id=1, replica_groups=mesh['sp'=8,'tp'=4] {'sp'}, dimensions={0}, use_global_device_ids=true | all-gather | bytes 294912 | tf_op jit(solution)/shard_map/all_gather | solution.py:98
  44.7 1.0 fusion.14
  45.8 0.3 multiply_convert_fusion
  46.1 0.6 copy-done.2
  46.7 0.5 multiply_reduce_fusion.2
  47.2 0.6 slice_convert_fusion.3
  47.9 0.6 fusion.69
  48.5 4.7 %collective-permute-done.1 = bf16[2,256,64]{1,2,0:T(8,128)(2,1)S(1)} collective-permute-done((bf16[2,256,64]{1,2,0:T(8,128)(2,1)S(1)}, bf16[2,256,64]{1,2,0:T(8,128)(2,1)S(1)}, u32[]{:S(2)}, u32[]{:S(2)}) %collective-permute-start.1) | collective-permute-done | bytes 65568 | tf_op jit(solution)/shard_map/ppermute | solution.py:24
  53.5 6.6 %collective-permute-done.2 = bf16[4,256,64]{1,0,2:T(4,128)(2,1)S(1)} collective-permute-done((bf16[4,256,64]{1,0,2:T(4,128)(2,1)S(1)}, bf16[4,256,64]{1,0,2:T(4,128)(2,1)S(1)}, u32[]{:S(2)}, u32[]{:S(2)}) %collective-permute-start.2) | collective-permute-done | bytes 131104 | tf_op jit(solution)/shard_map/ppermute | solution.py:24
  60.3 0.2 reverse_select_fusion
  60.5 0.2 reshape_reshape.3
  60.6 0.4 fusion.23
  61.2 30.3 %all_gather.23 = bf16[2,1024,128]{1,2,0:T(8,128)(2,1)} all-gather(bf16[2,128,128]{1,2,0:T(8,128)(2,1)S(1)} %pad_maximum_fusion.6), channel_id=1, replica_groups=mesh['sp'=8,'tp'=4] {'sp'}, dimensions={1}, use_global_device_ids=true | all-gather | bytes 589824 | tf_op jit(solution)/shard_map/all_gather | solution.py:134
  91.5 1.5 copy.51
  93.0 0.5 multiply_reduce_fusion.1
  93.8 0.8 copy.99
  94.5 7.3 %conditional.1 = ((f32[2,1,512]{2,0,1:T(2,128)S(1)}, f32[2,1,512,64]{2,3,0,1:T(8,128)S(1)})) conditional(s32[]{:T(128)} %convert_element_type.126, (f32[2,1,512]{2,0,1:T(2,128)S(1)}, f32[2,1,512,64]{2,3,0,1:T(8,128)S(1)}) %tuple.30, (s32[]{:T(128)}, s32[4,128]{1,0:T(4,128)S(1)}, bf16[2,1,4,128,64]{3,2,4,0,1:T(4,128)(2,1)}, ...), branch_computations={%region_3.4_spmd, %region_4.0_spmd} | conditional | flops 281680384 | bytes 17967226 | solution.py:180
  94.6 0.9 dynamic-slice_bitcast_fusion
  95.4 1.0 reshape.368
  96.4 0.4 iota_compare_fusion
  96.8 2.4 %fusion.3 = (f32[2,512]{1,0:T(2,128)S(1)}, f32[2,512,1024]{2,1,0:T(8,128)S(1)}) fusion(f32[2,4,1024]{2,1,0:T(4,128)} %get-tuple-element.151, f32[2,512]{1,0:T(2,128)S(1)} %bitcast.193, pred[512,1024]{1,0:T(8,128)(4,1)S(1)} %iota_compare_fusion, bf16[2,512,64]{1,2,0:T(8,128)(2,1)S(1)} %reshape.368, bf16[2,1024,128]{1,2,0:T(8,128)(2,1)} %get-tuple-element.143), kind=kOutput, calls=%fused_computation.5 | convolution fusion | flops 139459584 | bytes 5152768 | tf_op jit(solution)/shard_map/while/body/eval_jaxpr/cond/branch_1_fun/bhqd,bkhd->bhqk/dot_general | solution.py:152
  99.2 1.8 fusion.1
  101.1 0.8 fusion.4
  101.9 0.7 broadcast_divide_fusion
  102.6 1.0 reshape.385
  103.6 0.2 fusion.42
  103.8 0.9 copy.57
  104.7 1.7 convolution_convert_fusion
  106.5 2.4 %collective-permute-start.3 = (bf16[2,3,256]{2,1,0:T(4,128)(2,1)S(1)}, bf16[2,3,256]{2,1,0:T(4,128)(2,1)S(1)}, u32[]{:S(2)}, u32[]{:S(2)}) collective-permute-start(bf16[2,3,256]{2,1,0:T(4,128)(2,1)S(1)} %slice.399), channel_id=1, source_target_pairs={{0,4},{4,8},{8,12},{12,16},{16,20},{20,24},{24,28},{1,5},{5,9},{9,... | collective-permute-start | bytes 9224 | tf_op jit(solution)/shard_map/ppermute | solution.py:38
  109.1 1.8 fusion.76
  111.3 0.3 fusion.18
  111.8 0.3 fusion.22
  112.2 0.2 convert_multiply_fusion
  115.0 26.2 %all-gather = f32[16,1,256]{2,1,0:T(1,128)S(1)} all-gather(f32[2,1,256]{2,1,0:T(1,128)S(1)} %slice_add_fusion.4), channel_id=2, replica_groups=mesh['sp'=8,'tp'=4] {'sp'}, dimensions={0}, use_global_device_ids=true | all-gather | bytes 18432 | tf_op jit(solution)/shard_map/all_gather | solution.py:221
  141.5 26.1 %all-gather.1 = f32[16,1,256]{2,1,0:T(1,128)S(1)} all-gather(f32[2,1,256]{2,1,0:T(1,128)S(1)} %slice_add_fusion.3), channel_id=3, replica_groups=mesh['sp'=8,'tp'=4] {'sp'}, dimensions={0}, use_global_device_ids=true | all-gather | bytes 18432 | tf_op jit(solution)/shard_map/all_gather | solution.py:220
  168.1 2.4 %fusion.75 = (f32[2,128,256]{2,1,0:T(8,128)}, f32[2,128,256]{2,1,0:T(8,128)S(1)}) fusion(bf16[2,128,2048]{2,1,0:T(8,128)(2,1)S(1)} %multiply_convert_fusion, bf16[2048,256]{1,0:T(8,128)(2,1)} %all-gather.10.cloned.1.call-done, f32[2,256]{1,0:T(2,128)S(1)} %fusion.67, f32[2,128,256]{2,1,0:T(8,128)S(1)} %pad.131, f32[2,128,256]{2,1,0:T(8,128)S(1)} %pad.132, ...), kind=kOutput, calls=%fused_computation.178 | convolution fusion | flops 269352960 | bytes 3672064 | tf_op jit(solution)/shard_map/dot_general | solution.py:105
  170.5 1.9 copy.68
  172.4 1.9 mul.433
  174.3 1.0 reduce_sum.60
  175.3 0.8 copy.69
  176.1 1.0 fusion.41
  177.2 1.7 fusion.12
  178.9 1.1 copy.98
  180.0 22.5 %reduce-scatter.2.cloned.1.call-done = bf16[256,512]{1,0:T(8,128)(2,1)} async-done(((bf16[1024,512]{1,0:T(8,128)(2,1)}), bf16[256,512]{1,0:T(8,128)(2,1)}) %reduce-scatter.2.cloned.1.call-update) | async-done | bytes 262160 | tf_op jit(solution)/shard_map/reduce_scatter | solution.py:243
  (217 shorter events, 4.7 us)
Async XLA Ops:
  6.5 102.6 %copy-start = (bf16[256,2048]{1,0:T(8,128)(2,1)S(1)}, bf16[256,2048]{1,0:T(8,128)(2,1)}, u32[]{:S(2)}) copy-start(bf16[256,2048]{1,0:T(8,128)(2,1)} %param.38) | copy-start | bytes 3145732
  6.5 38.2 %copy-start.1 = (bf16[2,128,2048]{2,1,0:T(8,128)(2,1)S(1)}, bf16[2,128,2048]{2,1,0:T(8,128)(2,1)}, u32[]{:S(2)}) copy-start(bf16[2,128,2048]{2,1,0:T(8,128)(2,1)} %param.21) | copy-start | bytes 3145732
  6.5 39.2 %copy-start.9 = (f32[2048]{0:T(1024)S(1)}, f32[2048]{0:T(1024)}, u32[]{:S(2)}) copy-start(f32[2048]{0:T(1024)} %param.22) | copy-start | bytes 24580
  6.5 85.0 %all-gather.6.cloned.1.call-start = ((), (), s32[]{:S(2)}) async-start(), calls=%async_computation.1 | async-start | bytes 1179648 | tf_op jit(solution)/shard_map/all_gather | solution.py:97
  7.3 97.5 %all-gather.8.cloned.1.call-start = ((), (), s32[]{:S(2)}) async-start(), calls=%async_computation.2 | async-start | bytes 1179648 | tf_op jit(solution)/shard_map/all_gather | solution.py:100
  8.0 160.0 %all-gather.10.cloned.1.call-start = ((), (), s32[]{:S(2)}) async-start(), calls=%async_computation.3 | async-start | bytes 1179648 | tf_op jit(solution)/shard_map/all_gather | solution.py:101
  8.1 39.7 %collective-permute-start = (bf16[1,256,64]{1,2,0:T(8,128)(2,1)}, bf16[1,256,64]{1,2,0:T(8,128)(2,1)S(1)}, u32[]{:S(2)}, u32[]{:S(2)}) collective-permute-start(bf16[1,256,64]{1,2,0:T(8,128)(2,1)} %bitcast.200), channel_id=1, source_target_pairs={{0,4},{4,0},{8,12},{12,8},{16,20},{20,16},{24,28},{28,24},{1,5},{5... | collective-permute-start | bytes 98312 | tf_op jit(solution)/shard_map/ppermute | solution.py:24
  11.1 191.3 %reduce-scatter.2.cloned.1.call-start = ((), (), s32[]{:S(2)}) async-start(), calls=%async_computation.4 | async-start | bytes 1310720 | tf_op jit(solution)/shard_map/reduce_scatter | solution.py:243
  45.7 1.0 copy-start.2
  45.7 1.4 copy-start.11
  45.7 2.0 copy-start.10
  45.7 2.1 %copy-start.19 = (f32[256]{0:T(256)S(1)}, f32[256]{0:T(256)}, u32[]{:S(2)}) copy-start(f32[256]{0:T(256)} %param.34) | copy-start | bytes 3076
  47.8 5.4 %collective-permute-start.1 = (bf16[2,256,64]{1,2,0:T(8,128)(2,1)S(1)}, bf16[2,256,64]{1,2,0:T(8,128)(2,1)S(1)}, u32[]{:S(2)}, u32[]{:S(2)}) collective-permute-start(bf16[2,256,64]{1,2,0:T(8,128)(2,1)S(1)} %get-tuple-element.169), channel_id=1, source_target_pairs={{0,8},{4,12},{8,0},{12,4},{16,24},{20,28},{24,16},{28,20},{1,9},{5... | collective-permute-start | bytes 196616 | tf_op jit(solution)/shard_map/ppermute | solution.py:24
  48.5 12.6 %copy-start.20 = (f32[64]{0:T(128)S(1)}, f32[64]{0:T(128)}, u32[]{:S(2)}) copy-start(f32[64]{0:T(128)} %param.27) | copy-start | bytes 772
  53.3 6.8 %collective-permute-start.2 = (bf16[4,256,64]{1,0,2:T(4,128)(2,1)S(1)}, bf16[4,256,64]{1,0,2:T(4,128)(2,1)S(1)}, u32[]{:S(2)}, u32[]{:S(2)}) collective-permute-start(bf16[4,256,64]{1,0,2:T(4,128)(2,1)S(1)} %copy.53), channel_id=1, source_target_pairs={{0,16},{4,20},{8,24},{12,28},{16,0},{20,4},{24,8},{28,12},{1,17},{... | collective-permute-start | bytes 393224 | tf_op jit(solution)/shard_map/ppermute | solution.py:24
  93.0 0.7 copy-start.21
  94.5 10.2 %copy-start.3 = (bf16[256,2048]{1,0:T(8,128)(2,1)S(1)}, bf16[256,2048]{1,0:T(8,128)(2,1)}, u32[]{:S(2)}) copy-start(bf16[256,2048]{1,0:T(8,128)(2,1)} %copy-done.2) | copy-start | bytes 3145732
  96.7 2.5 %copy-start.8 = (f32[2,4,1024]{2,1,0:T(4,128)S(1)}, f32[2,4,1024]{2,1,0:T(4,128)}, u32[]{:S(2)}) copy-start(f32[2,4,1024]{2,1,0:T(4,128)} %get-tuple-element.151) | copy-start | bytes 98308 | tf_op jit(solution)/shard_map/while/body/eval_jaxpr/cond
  99.2 1.8 copy-start.5
  101.9 7.1 %copy-start.17 = (f32[256]{0:T(256)S(1)}, f32[256]{0:T(256)}, u32[]{:S(2)}) copy-start(f32[256]{0:T(256)} %param.36) | copy-start | bytes 3076
  104.7 4.2 %copy-start.6 = (f32[2,1,4,128,64]{3,0,4,2,1:T(2,128)S(1)}, f32[2,1,4,128,64]{3,0,4,2,1:T(2,128)}, u32[]{:S(2)}) copy-start(f32[2,1,4,128,64]{3,0,4,2,1:T(2,128)} %copy.57) | copy-start | bytes 786436
  106.5 4.5 %copy-start.13 = (f32[1,256]{1,0:T(1,128)S(1)}, f32[1,256]{1,0:T(1,128)}, u32[]{:S(2)}) copy-start(f32[1,256]{1,0:T(1,128)} %get-tuple-element.201) | copy-start | bytes 3076
  106.5 4.4 %copy-start.14 = (f32[1,256]{1,0:T(1,128)S(1)}, f32[1,256]{1,0:T(1,128)}, u32[]{:S(2)}) copy-start(f32[1,256]{1,0:T(1,128)} %get-tuple-element.202) | copy-start | bytes 3076
  106.5 4.4 %copy-start.15 = (f32[1,256]{1,0:T(1,128)S(1)}, f32[1,256]{1,0:T(1,128)}, u32[]{:S(2)}) copy-start(f32[1,256]{1,0:T(1,128)} %get-tuple-element.203) | copy-start | bytes 3076
  106.5 4.4 %copy-start.16 = (f32[1,256]{1,0:T(1,128)S(1)}, f32[1,256]{1,0:T(1,128)}, u32[]{:S(2)}) copy-start(f32[1,256]{1,0:T(1,128)} %get-tuple-element.204) | copy-start | bytes 3076
  106.5 4.4 %collective-permute-start.3 = (bf16[2,3,256]{2,1,0:T(4,128)(2,1)S(1)}, bf16[2,3,256]{2,1,0:T(4,128)(2,1)S(1)}, u32[]{:S(2)}, u32[]{:S(2)}) collective-permute-start(bf16[2,3,256]{2,1,0:T(4,128)(2,1)S(1)} %slice.399), channel_id=1, source_target_pairs={{0,4},{4,8},{8,12},{12,16},{16,20},{20,24},{24,28},{1,5},{5,9},{9,... | collective-permute-start | bytes 9224 | tf_op jit(solution)/shard_map/ppermute | solution.py:38
  109.0 2.3 %copy-start.22 = (bf16[4,64,64]{2,1,0:T(8,128)(2,1)S(1)}, bf16[4,64,64]{2,1,0:T(8,128)(2,1)}, u32[]{:S(2)}) copy-start(bf16[4,64,64]{2,1,0:T(8,128)(2,1)} %param.33) | copy-start | bytes 98308
  110.9 0.8 copy-start.23
  111.2 1.0 copy-start.7
  111.2 1.0 copy-start.12
  168.0 8.1 %copy-start.18 = (f32[256]{0:T(256)S(1)}, f32[256]{0:T(256)}, u32[]{:S(2)}) copy-start(f32[256]{0:T(256)} %param.37) | copy-start | bytes 3076
  170.5 6.7 %copy-start.4 = (f32[256,2048]{1,0:T(8,128)S(1)}, f32[256,2048]{1,0:T(8,128)}, u32[]{:S(2)}) copy-start(f32[256,2048]{1,0:T(8,128)} %fusion.76) | copy-start | bytes 6291460
Sparse Core Ops, SparseCore 0:
  9.5 44.6 all-gather.5
  56.3 41.4 all-gather.7
  99.9 38.7 all-gather.9
  180.1 22.3 reduce-scatter.1
